TPU v7x, 32 devices: a whole 2x2x4 slice. The times are simulated.
32 devices in a mesh: sp: 8 (over z, y), tp: 4 (over x, core).
Axes of the slice: x: 2, y: 2, z: 4, core: 2. Of those that a mesh axis runs over, the one named last changes fastest.
Arguments:
- tokens: bfloat16 [4096, 2048], P(('sp', 'tp')), may hold values from -8 to 8, as said below
- w_query: bfloat16 [2048, 1024], P(None, 'tp'), may hold values from -0.125 to 0.125
- w_key: bfloat16 [2048, 1024], P(None, 'tp'), may hold values from -0.125 to 0.125
- w_value: bfloat16 [2048, 1024], P(None, 'tp'), may hold values from -0.125 to 0.125
- head_bias: float32 [16], P('tp'), may hold values from -40 to -3
- w_out: bfloat16 [1024, 2048], P('tp'), may hold values from -0.1875 to 0.1875
Outputs:
- mixed: bfloat16 [4096, 2048], P(('sp', 'tp'))
Inputs may be any that keep to these rules, and one draw needn't show every extreme that they name: `tokens`: activations of order one whose mean shifts between blocks of 512 positions.
All inputs are finite; a program needn't handle non-finite values.
Results may differ from a plain program's by a relative error of at most 0.014.
Values may be sent and summed in bfloat16 or wider, within the bound.
A program may use at most 128 MiB of HBM per device.

v0:
```python
import jax
import jax.numpy as jnp
from jax import lax
from jax.sharding import PartitionSpec as P


def segment_terms(query_rows, query_pos, key_span, value_span, key_pos, bias):
    head_size = query_rows.shape[2]
    scores = jnp.einsum("rhd,sthd->rhst", query_rows, key_span, preferred_element_type=jnp.float32)
    scores = scores * head_size ** (-0.5) + bias[None, :, None, None]
    causal = key_pos[None, None] < query_pos[:, None, None, None]
    log_keep = jnp.where(causal, jax.nn.log_sigmoid(-scores), 0.0)
    tail = lax.cumsum(log_keep, axis=3, reverse=True) - log_keep
    weights = jnp.where(causal, jnp.exp(jax.nn.log_sigmoid(scores) + tail), 0.0).astype(
        jnp.bfloat16
    )
    segment_out = jnp.einsum(
        "rhst,sthd->rhsd", weights, value_span, preferred_element_type=jnp.float32
    )
    segment_total = jnp.sum(log_keep, axis=3)
    return (segment_out, segment_total)


def shards(tokens, w_query, w_key, w_value, head_bias, w_out):
    local_width = w_query.shape[1]
    heads_here = head_bias.shape[0]
    head_size = local_width // heads_here
    joined = jnp.concatenate([w_query, w_key, w_value], axis=1)
    projected = jnp.dot(
        lax.all_gather(tokens, "tp", axis=0, tiled=True), joined, preferred_element_type=jnp.float32
    ).astype(jnp.bfloat16)
    own_rows = projected.shape[0]
    queries = projected[:, :local_width]
    keys_local = projected[:, local_width : 2 * local_width]
    values_local = projected[:, 2 * local_width :]
    seq_count = lax.axis_size("sp")
    seq_index = lax.axis_index("sp")
    span_segments = max(
        (
            divisor
            for divisor in range(1, seq_count + 1)
            if seq_count % divisor == 0 and divisor * own_rows <= max(1024, own_rows)
        )
    )
    span_length = span_segments * own_rows
    query_rows_all = lax.all_gather(queries, "sp", axis=0, tiled=True)
    total_rows = query_rows_all.shape[0]
    query_all = query_rows_all.reshape(total_rows, heads_here, head_size)
    key_span = keys_local.reshape(1, own_rows, heads_here, head_size)
    value_span = values_local.reshape(1, own_rows, heads_here, head_size)
    key_pos = (seq_index * own_rows + jnp.arange(own_rows, dtype=jnp.int32)).reshape(1, own_rows)
    block_total = total_rows // span_length
    first_block = seq_index * own_rows // span_length

    def visit(block_index, buffers):
        out_buffer, keep_buffer = buffers
        first_row = block_index * span_length
        query_block = lax.dynamic_slice_in_dim(query_all, first_row, span_length, 0)
        query_pos = first_row + jnp.arange(span_length, dtype=jnp.int32)
        segment_out, segment_total = segment_terms(
            query_block, query_pos, key_span, value_span, key_pos, head_bias
        )
        out_buffer = lax.dynamic_update_slice_in_dim(
            out_buffer, segment_out[:, :, 0, :].reshape(span_length, local_width), first_row, 0
        )
        keep_buffer = lax.dynamic_update_slice_in_dim(
            keep_buffer, segment_total[:, :, 0], first_row, 0
        )
        return (out_buffer, keep_buffer)

    out_buffer, keep_buffer = lax.fori_loop(
        first_block,
        block_total,
        visit,
        (
            jnp.zeros((total_rows, local_width), jnp.float32),
            jnp.zeros((total_rows, heads_here), jnp.float32),
        ),
    )
    keep_sent = jnp.transpose(keep_buffer.reshape(seq_count, own_rows, heads_here), (0, 2, 1))
    received_out, received_keep = (
        lax.all_to_all(
            out_buffer.reshape(seq_count, own_rows, local_width),
            "sp",
            split_axis=0,
            concat_axis=0,
            tiled=True,
        ),
        lax.all_to_all(keep_sent, "sp", split_axis=0, concat_axis=0, tiled=True),
    )
    keep_rows = jnp.transpose(received_keep, (0, 2, 1))
    later = lax.cumsum(keep_rows, axis=0, reverse=True) - keep_rows
    pieces = received_out.reshape(seq_count, own_rows, heads_here, head_size)
    attended = jnp.sum(jnp.exp(later)[..., None] * pieces, axis=0).astype(jnp.bfloat16)
    attended_rows = attended.reshape(own_rows, local_width)
    return lax.psum_scatter(
        jnp.dot(attended_rows, w_out, preferred_element_type=jnp.float32).astype(jnp.bfloat16),
        "tp",
        scatter_dimension=0,
        tiled=True,
    )


def solution(mesh):
    placed = (
        P(("sp", "tp"), None),
        P(None, "tp"),
        P(None, "tp"),
        P(None, "tp"),
        P("tp"),
        P("tp", None),
    )
    return jax.shard_map(
        shards, mesh=mesh, in_specs=placed, out_specs=P(("sp", "tp"), None), check_vma=False
    )
```

profile of v0, /device:TPU:29, one launch (start us, length us, event | category | flops | bytes accessed | tf_op | source)
XLA Modules:
  0.0 602.2 jit_solution(7391056400099784817)
XLA Ops:
  6.5 0.7 all-gather.3.cloned.1.call-update
  7.3 25.5 %all-gather.3.cloned.1.call-done = bf16[512,2048]{1,0:T(8,128)(2,1)} async-done(((bf16[128,2048]{1,0:T(8,128)(2,1)}), bf16[512,2048]{1,0:T(8,128)(2,1)}) %all-gather.3.cloned.1.call-update) | async-done | bytes 2097168 | tf_op jit(solution)/shard_map/all_gather | solution.py:30
  32.8 4.4 fusion.31
  37.2 0.8 fusion.38
  38.1 47.3 %all-gather.5.cloned.1.call-done = bf16[4096,256]{0,1:T(8,128)(2,1)} async-done(((bf16[512,256]{0,1:T(8,128)(2,1)}), bf16[4096,256]{0,1:T(8,128)(2,1)}) %all-gather.5.cloned.1.call-update) | async-done | bytes 2097168 | tf_op jit(solution)/shard_map/all_gather | solution.py:46
  85.3 0.6 broadcast_in_dim.24
  86.0 2.2 broadcast_in_dim.23.clone
  88.2 93.4 %while.13 = (s32[]{:T(128)}, f32[4096,256]{1,0:T(8,128)}, f32[4096,4]{0,1:T(4,128)}, bf16[4096,4,64]{0,2,1:T(8,128)(2,1)}, bf16[1,512,4,64]{1,3,2,0:T(8,128)(2,1...) while((s32[]{:T(128)}, f32[4096,256]{1,0:T(8,128)}, ...), condition=%wide.region_4.5_spmd.clone, body=%wide.region_0.4_spmd.clone.sunk | while | flops 875095552 | bytes 83898592 | solution.py:71
  88.5 0.4 broadcast_compare_fusion.2
  88.9 13.4 %fusion.52 = (f32[1024,4]{0,1:T(4,128)S(1)}, f32[1024,4,1,512]{0,3,1,2:T(8,128)}, f32[4,1024,512]{1,2,0:T(8,128)}) fusion(f32[4]{0:T(128)S(1)} %get-tuple-element.177, pred[1024,512]{0,1:T(8,128)(4,1)S(1)} %broadcast_compare_fusion.2, bf16[1,512,4,64]{1,3,2,0:T(8,128)(2,1)} %get-tuple-element.176, bf16[4096,4,64]{0,2,1:T(8,128)(2,1)} %get-tuple-element.175, ...), kind=kOutput, calls=%fused_computation.30.clone.1 | convolution fusion | flops 291500032 | bytes 18104340 | tf_op jit(solution)/shard_map/while/body/rhd,sthd->rhst/dot_general | solution.py:9
  102.3 48.9 %fusion.53 = f32[1024,4,1,4,128]{0,3,2,1,4:T(4,128)S(1)} fusion(f32[1024,4,1,4,128]{0,4,3,1,2:T(8,128)} %bitcast.100), kind=kOutput, calls=%fused_computation.14.clone.1 | output fusion | flops 266338304 | bytes 16777216 | tf_op jit(solution)/shard_map/reduce-window
  151.3 8.1 %copy.32 = f32[1024,4,1,4,128]{0,4,3,1,2:T(8,128)} copy(f32[1024,4,1,4,128]{0,3,2,1,4:T(4,128)S(1)} %fusion.53) | data formatting | bytes 16777216 | tf_op jit(solution)/shard_map/reduce-window
  159.5 15.9 %fusion.54 = bf16[1024,4,1,512]{0,3,1,2:T(8,128)(2,1)S(1)} fusion(f32[1024,4,1,4,128]{0,4,3,1,2:T(8,128)} %copy.32, f32[4,1024,512]{1,2,0:T(8,128)} %get-tuple-element.144, f32[1024,4,4]{0,2,1:T(4,128)S(1)} %slice_bitcast_fusion.5, f32[4]{0:T(128)S(1)} %get-tuple-element.177, pred[1024,512]{0,1:T(8,128)(4,1)S(1)} %broadcast_compare_fusion.2), kind=kLoop, calls=%fused_computation.7.clone.1 | loop fusion | flops 48234496 | bytes 21561360 | tf_op jit(solution)/shard_map/while/body/convert_element_type | solution.py:14
  175.4 0.9 fusion.55
  176.3 0.3 copy.33
  176.6 0.6 constant_dynamic-update-slice_fusion.5
  177.2 1.1 constant_dynamic-update-slice_fusion.4
  181.5 274.7 %all-to-all-start = ((f32[8,4,512]{2,1,0:T(4,128)}), f32[8,4,512]{2,1,0:T(4,128)S(1)}, u32[]{:S(2)}, u32[]{:S(2)}) async-start(f32[8,4,512]{2,1,0:T(4,128)} %bitcast.5), calls=%async_computation | async-start | bytes 131072 | tf_op jit(solution)/shard_map/all_to_all | solution.py:89
  456.3 5.4 copy.18
  461.6 5.4 all-to-all-start.1
  467.1 91.6 %all-to-all-done.1 = f32[8,512,256]{1,2,0:T(8,128)} async-done(((f32[8,512,256]{1,2,0:T(8,128)}), f32[8,512,256]{1,2,0:T(8,128)}, u32[]{:S(2)}, u32[]{:S(2)}) %all-to-all-start.1) | async-done | bytes 4194336 | tf_op jit(solution)/shard_map/all_to_all | solution.py:82
  558.7 2.7 fusion.21
  561.5 2.1 convolution_convert_fusion
  563.6 31.9 %reduce-scatter.2.cloned.1.call-done = bf16[128,2048]{1,0:T(8,128)(2,1)} async-done(((bf16[512,2048]{1,0:T(8,128)(2,1)}), bf16[128,2048]{1,0:T(8,128)(2,1)}) %reduce-scatter.2.cloned.1.call-update) | async-done | bytes 524304 | tf_op jit(solution)/shard_map/reduce_scatter | solution.py:96
  (16 shorter events, 0.3 us)
Async XLA Ops:
  6.5 554.9 %copy-start = (bf16[256,2048]{1,0:T(8,128)(2,1)S(1)}, bf16[256,2048]{1,0:T(8,128)(2,1)}, u32[]{:S(2)}) copy-start(bf16[256,2048]{1,0:T(8,128)(2,1)} %param.13) | copy-start | bytes 3145732
  6.5 26.3 %all-gather.3.cloned.1.call-start = ((), (), s32[]{:S(2)}) async-start(), calls=%async_computation.3 | async-start | bytes 2621440 | tf_op jit(solution)/shard_map/all_gather | solution.py:30
  7.3 80.9 %copy-start.1 = (f32[4]{0:T(128)S(1)}, f32[4]{0:T(128)}, u32[]{:S(2)}) copy-start(f32[4]{0:T(128)} %param.12) | copy-start | bytes 52
  7.3 78.1 %all-gather.5.cloned.1.call-start = ((), (), s32[]{:S(2)}) async-start(), calls=%async_computation.4 | async-start | bytes 2359296 | tf_op jit(solution)/shard_map/all_gather | solution.py:46
  181.5 280.1 %all-to-all-start = ((f32[8,4,512]{2,1,0:T(4,128)}), f32[8,4,512]{2,1,0:T(4,128)S(1)}, u32[]{:S(2)}, u32[]{:S(2)}) async-start(f32[8,4,512]{2,1,0:T(4,128)} %bitcast.5), calls=%async_computation | async-start | bytes 131072 | tf_op jit(solution)/shard_map/all_to_all | solution.py:89
  461.6 97.1 %all-to-all-start.1 = ((f32[8,512,256]{1,2,0:T(8,128)}), f32[8,512,256]{1,2,0:T(8,128)}, u32[]{:S(2)}, u32[]{:S(2)}) async-start(f32[8,512,256]{1,2,0:T(8,128)} %copy.18), calls=%async_computation.1 | async-start | bytes 8388608 | tf_op jit(solution)/shard_map/all_to_all | solution.py:82
  467.1 128.4 %reduce-scatter.2.cloned.1.call-start = ((), (), s32[]{:S(2)}) async-start(), calls=%async_computation.5 | async-start | bytes 2621440 | tf_op jit(solution)/shard_map/reduce_scatter | solution.py:96
Sparse Core Ops, SparseCore 0:
  8.9 23.8 all-gather.2
  38.2 47.1 all-gather.4
  563.7 31.7 reduce-scatter.1
where the time goes:
time: 607 us; the launch traced here: 602 us
  starting transfers between devices  280 us (46%)
  waiting for transfers between devices  197 us (32%)
  other arithmetic  68.1 us (11%)
  matrix products  20.8 us (3%)
  local copies, waits for them, and re-layouts  19.1 us (3%)
  between operations  13.4 us (2%)
    all_to_all x1, starting transfers between devices, shards(): lax.all_to_all(keep_sent, 'sp', split_axis=0, concat_axis=0, tiled=True)  275 us
    all_to_all x1, waiting for transfers between devices, shards(): lax.all_to_all(out_buffer.reshape(seq_count, own_rows, local_width), 'sp'...  91.6 us
    another operation x2, other arithmetic  49 us
    all_gather x1, waiting for transfers between devices, shards(): query_rows_all = lax.all_gather(queries, 'sp', axis=0, tiled=True)  47.3 us
    reduce_scatter x1, waiting for transfers between devices, shards(): lax.psum_scatter(jnp.dot(attended_rows, w_out, preferred_element_type=jnp...  31.9 us
    all_gather x1, waiting for transfers between devices, shards(): lax.all_gather(tokens, 'tp', axis=0, tiled=True)  25.5 us
    convert_element_type x1, other arithmetic, segment_terms(): jnp.where(causal, jnp.exp(jax.nn.log_sigmoid(scores) + tail), 0.0)  15.9 us
    dot_general x1, matrix products, segment_terms(): jnp.einsum('rhd,sthd->rhst', query_rows, key_span, preferred_element_type...  13.4 us
  transfers between devices with their start and end apart: 5, of which 4 were waited for; matrix products, arithmetic and copies ran while one was open for 1% of the time, Pallas kernels for 0%

commit v1 on v0

v1 whole, which is shorter than its diff:
```python
import functools
import math

import jax
import jax.numpy as jnp
from jax import lax
from jax.experimental import pallas as pl
from jax.experimental.pallas import tpu as pltpu
from jax.sharding import PartitionSpec as P

MESH = pl.DeviceIdType.MESH
LOG2E = math.log2(math.e)
CHUNK = 256


def attention_kernel(
    n_sp, n_tp, heads, piece, bias_ref, q_ref, kv_ref, out_ref,
    q_all, kv_all, packed, tri, send_sem, recv_sem, local_sem, back_send, back_recv
):
    me = lax.axis_index("sp")
    col = lax.axis_index("tp")
    share_count = n_sp // heads
    seg = kv_ref.shape[1]
    width = kv_ref.shape[2]
    half = width // 2
    rows = q_ref.shape[2] * 2
    pieces = rows // piece
    my_head = me // share_count
    my_share = lax.rem(me, share_count)

    barrier = pltpu.get_barrier_semaphore()
    total = n_sp * n_tp
    flat = me * n_tp + col

    def greet(step, carry):
        other = lax.rem(flat + step, total)
        pl.semaphore_signal(
            barrier, inc=1, device_id=(other // n_tp, lax.rem(other, n_tp)), device_id_type=MESH
        )
        return carry

    lax.fori_loop(1, total, greet, 0)

    key_id = lax.broadcasted_iota(jnp.int32, (CHUNK, CHUNK), 0)
    out_id = lax.broadcasted_iota(jnp.int32, (CHUNK, CHUNK), 1)
    tri[...] = jnp.where(key_id > out_id, 1.0, 0.0).astype(jnp.bfloat16)
    own = [
        pltpu.make_async_copy(kv_ref.at[my_head], kv_all.at[me], local_sem.at[0]),
        pltpu.make_async_copy(
            q_ref.at[my_head, lax.rem(my_share + me, share_count)], q_all.at[me], local_sem.at[1]
        ),
    ]
    for copy in own:
        copy.start()
    pl.semaphore_wait(barrier, total - 1)

    def outgoing(step):
        peer = lax.rem(me + step, n_sp)
        head = peer // share_count
        share = lax.rem(lax.rem(peer, share_count) + me, share_count)
        return (
            pltpu.make_async_remote_copy(
                src_ref=kv_ref.at[head], dst_ref=kv_all.at[me],
                send_sem=send_sem.at[0, step], recv_sem=recv_sem.at[0, me],
                device_id=(peer, col), device_id_type=MESH,
            ),
            pltpu.make_async_remote_copy(
                src_ref=q_ref.at[head, share], dst_ref=q_all.at[me],
                send_sem=send_sem.at[1, step], recv_sem=recv_sem.at[1, me],
                device_id=(peer, col), device_id_type=MESH,
            ),
        )

    for step in range(1, n_sp):
        for copy in outgoing(step):
            copy.start()
    for copy in own:
        copy.wait()

    bias = bias_ref[0] * LOG2E
    lane = lax.broadcasted_iota(jnp.int32, (rows // 2, width), 1)

    def chunk_terms(q, keys, offset, row_first, state, diagonal):
        acc, later = state
        scores = lax.dot_general(
            q, keys, (((1,), (1,)), ((), ())), preferred_element_type=jnp.float32
        )
        z = scores * LOG2E + bias
        log_take = jnp.minimum(z, 0.0) - jnp.log2(1.0 + jnp.exp2(-jnp.abs(z)))
        keep = log_take - z
        if diagonal:
            q_pos = row_first + lax.broadcasted_iota(jnp.int32, z.shape, 0)
            k_pos = offset + lax.broadcasted_iota(jnp.int32, z.shape, 1)
            live = k_pos < q_pos
            keep = jnp.where(live, keep, 0.0)
        keep16 = keep.astype(jnp.bfloat16)
        tail = jnp.dot(keep16, tri[...], preferred_element_type=jnp.float32)
        weight = jnp.exp2(log_take + tail + later)
        if diagonal:
            weight = jnp.where(live, weight, 0.0)
        acc = acc + jnp.dot(
            weight.astype(jnp.bfloat16), keys, preferred_element_type=jnp.float32
        )
        later = later + (tail[:, 0:1] + keep16[:, 0:1].astype(jnp.float32))
        return acc, later

    def back(block, index, first_row):
        owner = first_row // piece + index
        return pltpu.make_async_remote_copy(
            src_ref=packed.at[block, index], dst_ref=out_ref.at[col * heads + my_head],
            send_sem=back_send.at[block, index], recv_sem=back_recv.at[col * heads + my_head],
            device_id=(block, owner), device_id_type=MESH,
        )

    def visit(block, carry):
        @pl.when(block != me)
        def _():
            for part, dst in ((0, kv_all), (1, q_all)):
                pltpu.make_async_copy(dst.at[block], dst.at[block], recv_sem.at[part, block]).wait()

        pair = q_all[block]
        zero = jnp.zeros_like(pair)
        low = jnp.where(lane < half, pair, zero)
        high = pltpu.roll(pair.astype(jnp.float32), half, 1).astype(pair.dtype)
        high = jnp.where(lane < half, high, zero)
        q = jnp.concatenate([low, high], axis=0)
        first_row = lax.rem(my_share + block, share_count) * rows

        state = (jnp.zeros((rows, width), jnp.float32), jnp.zeros((rows, 1), jnp.float32))
        for index in reversed(range(seg // CHUNK)):
            keys = kv_all[block, pl.ds(index * CHUNK, CHUNK), :]
            state = chunk_terms(q, keys, index * CHUNK, first_row, state, True)

        def earlier(step, state):
            segment = block - 1 - step
            for index in reversed(range(seg // CHUNK)):
                keys = kv_all[segment, pl.ds(index * CHUNK, CHUNK), :]
                state = chunk_terms(q, keys, index * CHUNK, 0, state, False)
            return state

        acc, _ = lax.fori_loop(0, block, earlier, state)
        for index in range(pieces):
            top = acc[index * piece : index * piece + piece // 2]
            bottom = acc[index * piece + piece // 2 : (index + 1) * piece]
            lanes = lax.broadcasted_iota(jnp.int32, top.shape, 1)
            folded = jnp.where(lanes < half, pltpu.roll(top, half, 1), bottom)
            packed[block, index] = folded.astype(jnp.bfloat16)
            owner = first_row // piece + index
            here = jnp.logical_and(block == me, owner == col)

            @pl.when(here)
            def _():
                out_ref[col * heads + my_head] = folded.astype(jnp.bfloat16)

            @pl.when(jnp.logical_not(here))
            def _():
                back(block, index, first_row).start()

        return carry

    lax.fori_loop(0, n_sp, visit, 0)

    for step in range(1, n_sp):
        for copy in outgoing(step):
            copy.wait_send()

    def drain(block, carry):
        first_row = lax.rem(my_share + block, share_count) * rows
        for index in range(pieces):
            owner = first_row // piece + index

            @pl.when(jnp.logical_not(jnp.logical_and(block == me, owner == col)))
            def _():
                back(block, index, first_row).wait_send()

        return carry

    lax.fori_loop(0, n_sp, drain, 0)

    share = (col * piece) // rows
    source_share = lax.rem(share + n_sp * share_count - me, share_count)
    for source_col in range(n_tp):
        for head in range(heads):
            slot = source_col * heads + head
            source = head * share_count + source_share

            @pl.when(jnp.logical_not(jnp.logical_and(source == me, source_col == col)))
            def _():
                pltpu.make_async_copy(
                    out_ref.at[slot], out_ref.at[slot], back_recv.at[slot]
                ).wait()


def shards(tokens, w_query, w_key, w_value, head_bias, w_out):
    local_width = w_query.shape[1]
    heads = head_bias.shape[0]
    head_size = local_width // heads
    n_sp = lax.axis_size("sp")
    n_tp = lax.axis_size("tp")
    device_rows = tokens.shape[0]
    own_rows = device_rows * n_tp
    share_count = n_sp // heads
    rows = own_rows // share_count
    width = 2 * head_size
    me = lax.axis_index("sp")

    gathered = lax.all_gather(tokens, "tp", axis=0, tiled=True)
    w_full = lax.all_gather(w_out, "tp", axis=0, tiled=True)
    joined = jnp.concatenate([w_query, w_key, w_value], axis=1)
    projected = jnp.dot(gathered, joined, preferred_element_type=jnp.float32)
    queries = (projected[:, :local_width] * head_size ** (-0.5)).astype(jnp.bfloat16)
    pairs = projected[:, local_width:].astype(jnp.bfloat16)
    kv = pairs.reshape(own_rows, 2, heads, head_size).transpose(2, 0, 1, 3)
    kv = kv.reshape(heads, own_rows, width)
    q = queries.reshape(share_count, 2, rows // 2, heads, head_size).transpose(3, 0, 2, 1, 4)
    q = q.reshape(heads, share_count, rows // 2, width)
    bias = lax.dynamic_slice_in_dim(head_bias, me // share_count, 1, 0)

    pieces = rows // device_rows
    vmem = pl.BlockSpec(memory_space=pltpu.VMEM)
    attended = pl.pallas_call(
        functools.partial(attention_kernel, n_sp, n_tp, heads, device_rows),
        out_shape=jax.ShapeDtypeStruct((n_tp * heads, device_rows // 2, width), jnp.bfloat16),
        in_specs=[pl.BlockSpec(memory_space=pltpu.SMEM), vmem, vmem],
        out_specs=vmem,
        scratch_shapes=[
            pltpu.VMEM((n_sp, rows // 2, width), jnp.bfloat16),
            pltpu.VMEM((n_sp, own_rows, width), jnp.bfloat16),
            pltpu.VMEM((n_sp, pieces, device_rows // 2, width), jnp.bfloat16),
            pltpu.VMEM((CHUNK, CHUNK), jnp.bfloat16),
            pltpu.SemaphoreType.DMA((2, n_sp)),
            pltpu.SemaphoreType.DMA((2, n_sp)),
            pltpu.SemaphoreType.DMA((2,)),
            pltpu.SemaphoreType.DMA((n_sp, pieces)),
            pltpu.SemaphoreType.DMA((n_tp * heads,)),
        ],
        compiler_params=pltpu.CompilerParams(collective_id=0, has_side_effects=True),
        cost_estimate=pl.CostEstimate(
            flops=4 * rows * n_sp * own_rows * n_sp * width, bytes_accessed=2**22, transcendentals=0
        ),
        name="attend",
    )(bias, q, kv)
    attended = attended.reshape(n_tp * heads, device_rows // 2, 2, head_size)
    attended = attended.transpose(2, 1, 0, 3).reshape(device_rows, n_tp * local_width)
    return jnp.dot(attended, w_full, preferred_element_type=jnp.float32).astype(jnp.bfloat16)


def solution(mesh):
    placed = (
        P(("sp", "tp"), None),
        P(None, "tp"),
        P(None, "tp"),
        P(None, "tp"),
        P("tp"),
        P("tp", None),
    )
    return jax.shard_map(
        shards, mesh=mesh, in_specs=placed, out_specs=P(("sp", "tp"), None), check_vma=False
    )
```

time: 607 us -> 117 us (0.19)
  starting transfers between devices: 280 us -> 0.04 us
  waiting for transfers between devices: 197 us -> 24.9 us
  other arithmetic: 68.1 us -> 0.04 us
  Pallas kernels: 0 us -> 64.6 us
  local copies, waits for them, and re-layouts: 19.1 us -> 5.25 us
  matrix products: 20.8 us -> 8.08 us
    all_to_all x2 -> x0, starting transfers between devices: 280 us -> none  [the longest x1 275 us: shards(): lax.all_to_all(keep_sent, 'sp', split_axis=0, concat_axis=0, tiled=True)]
    all_to_all x2 -> x0, waiting for transfers between devices: 91.6 us -> none  [the longest x1 91.6 us: shards(): lax.all_to_all(out_buffer.reshape(seq_count, own_rows, local_width), 'sp'...]
    pallas_call x0 -> x1, Pallas kernels: none -> 64.6 us  [shards(): pl.pallas_call(functools.partial(attention_kernel, n_sp, n_tp, heads, dev...]
    all_gather x2, waiting for transfers between devices: 72.8 us -> 23.5 us  [the longest x1 23.5 us: shards(): gathered = lax.all_gather(tokens, 'tp', axis=0, tiled=True)]
    another operation x3 -> x0, other arithmetic: 49.1 us -> none
    reduce_scatter x1 -> x0, waiting for transfers between devices: 31.9 us -> none  [shards(): lax.psum_scatter(jnp.dot(attended_rows, w_out, preferred_element_type=jnp...]
    convert_element_type x1, other arithmetic: 15.9 us -> 0.04 us  [shards(): (projected[:, :local_width] * head_size ** (-0.5)).astype(jnp.bfloat16)]
    dot_general x4 -> x2, matrix products: 20.8 us -> 8.08 us  [the longest x1 4.38 us: shards(): projected = jnp.dot(gathered, joined, preferred_element_type=jnp.float32)]
  transfers between devices with their start and end apart: 5 -> 2, of which waited for: 4 -> 1; matrix products, arithmetic and copies ran while one was open for 1% -> 8% of each run, Pallas kernels for 0% -> 55%
where the time goes in v1:
time: 117 us; the launch traced here: 116 us
  Pallas kernels  64.6 us (55%)
  waiting for transfers between devices  24.9 us (21%)
  between operations  13.5 us (12%)
  matrix products  8.08 us (7%)
  local copies, waits for them, and re-layouts  5.25 us (4%)
    pallas_call x1, Pallas kernels, shards(): pl.pallas_call(functools.partial(attention_kernel, n_sp, n_tp, heads, dev...  64.6 us
    all_gather x1, waiting for transfers between devices, shards(): gathered = lax.all_gather(tokens, 'tp', axis=0, tiled=True)  23.5 us
    dot_general x1, matrix products, shards(): projected = jnp.dot(gathered, joined, preferred_element_type=jnp.float32)  4.38 us
    dot_general x1, matrix products, shards(): jnp.dot(attended, w_full, preferred_element_type=jnp.float32)  3.7 us
  transfers between devices with their start and end apart: 2, of which 1 were waited for; matrix products, arithmetic and copies ran while one was open for 8% of the time, Pallas kernels for 55%

profile of v1, /device:TPU:29, one launch (start us, length us, event | category | flops | bytes accessed | tf_op | source)
XLA Modules:
  0.0 116.4 jit_solution(8472731789356145066)
XLA Ops:
  6.5 0.0 all-gather.3.cloned.1.call-start
  6.5 0.7 all-gather.3.cloned.1.call-update
  7.3 0.0 all-gather.5.cloned.1.call-start
  7.3 0.7 all-gather.5.cloned.1.call-update
  8.0 1.3 %dynamic_slice.3.bias_ref = f32[1]{0:T(128)} dynamic-slice(f32[4]{0:T(128)} %param.10, s32[]{:T(128)S(6)} %select_n.9), dynamic_slice_sizes={1} | dynamic-slice | bytes 12 | tf_op jit(solution)/shard_map/dynamic_slice | solution.py:217
  9.3 23.5 %all-gather.3.cloned.1.call-done = bf16[512,2048]{1,0:T(8,128)(2,1)} async-done(((bf16[128,2048]{1,0:T(8,128)(2,1)}), bf16[512,2048]{1,0:T(8,128)(2,1)}) %all-gather.3.cloned.1.call-update) | async-done | bytes 2097168 | tf_op jit(solution)/shard_map/all_gather | solution.py:207
  32.8 4.4 %fusion.6 = f32[512,768]{0,1:T(8,128)S(1)} fusion(bf16[512,2048]{1,0:T(8,128)(2,1)} %all-gather.3.cloned.1.call-done, bf16[2048,256]{1,0:T(8,128)(2,1)} %param.9, bf16[2048,256]{1,0:T(8,128)(2,1)} %param.8, bf16[2048,256]{1,0:T(8,128)(2,1)} %param.7), kind=kOutput, calls=%fused_computation.7 | convolution fusion | flops 1620049920 | bytes 6815744 | tf_op jit(solution)/shard_map/dot_general | solution.py:210
  37.2 0.1 slice.15
  37.3 1.0 copy.12.kv_ref
  38.4 0.1 reshape.18
  38.5 0.8 copy.11.q_ref
  39.3 64.6 %attend.1 = bf16[16,64,128]{2,1,0:T(8,128)(2,1)} custom-call(f32[1]{0:T(128)} %dynamic_slice.3.bias_ref, bf16[4,2,128,128]{3,2,1,0:T(8,128)(2,1)} %copy.11.q_ref, bf16[4,512,128]{2,1,0:T(8,128)(2,1)} %copy.12.kv_ref), custom_call_target="tpu_custom_call" | custom-call | flops 4294967296 | bytes 4194304 | tf_op jit(solution)/shard_map/attend/pallas_call | solution.py:221
  103.9 1.2 %reshape.22 = bf16[16,64,2,64]{3,2,1,0:T(2,128)(2,1)S(1)} reshape(bf16[16,64,128]{2,1,0:T(8,128)(2,1)} %attend.1) | data formatting | bytes 524288 | tf_op jit(solution)/shard_map/reshape | solution.py:243
  105.1 0.3 copy.15
  105.5 0.3 reshape.23
  105.8 0.0 all-gather.5.cloned.1.call-done
  105.8 3.7 %convolution_convert_fusion = bf16[128,2048]{1,0:T(8,128)(2,1)} fusion(bf16[128,1024]{1,0:T(8,128)(2,1)S(1)} %reshape.23, bf16[1024,2048]{1,0:T(8,128)(2,1)} %all-gather.5.cloned.1.call-done), kind=kOutput, calls=%fused_computation.6 | convolution fusion | flops 537133056 | bytes 4980736 | tf_op jit(solution)/shard_map/dot_general | solution.py:245
  (3 shorter events, 0.1 us)
Async XLA Ops:
  6.5 26.3 %all-gather.3.cloned.1.call-start = ((), (), s32[]{:S(2)}) async-start(), calls=%async_computation | async-start | bytes 2621440 | tf_op jit(solution)/shard_map/all_gather | solution.py:207
  7.3 98.6 %all-gather.5.cloned.1.call-start = ((), (), s32[]{:S(2)}) async-start(), calls=%async_computation.1 | async-start | bytes 5242880 | tf_op jit(solution)/shard_map/all_gather | solution.py:208
Sparse Core Ops, SparseCore 0:
  8.9 23.8 all-gather.2
  34.4 34.4 all-gather.4

commit v2 on v1

v2 whole, which is shorter than its diff:
```python
import functools
import math

import jax
import jax.numpy as jnp
from jax import lax
from jax.experimental import pallas as pl
from jax.experimental.pallas import tpu as pltpu
from jax.sharding import PartitionSpec as P

MESH = pl.DeviceIdType.MESH
LOG2E = math.log2(math.e)
CHUNK = 256
PARTS = 4
COLS = 512


def layer_kernel(
    n_sp, n_tp, heads, bias_ref, tokens_ref, wq_ref, wk_ref, wv_ref, wo_ref, out_ref,
    tok, wqkv, wfull, kv_own, q_own, q_all, kv_all, packed, att, att_rows, tri,
    load_sem, tok_send, tok_recv, wo_send, wo_recv, kv_send, kv_recv, q_send, q_recv,
    back_send, back_recv,
):
    me = lax.axis_index("sp")
    col = lax.axis_index("tp")
    share_count = n_sp // heads
    device_rows = PARTS * tokens_ref.shape[1]
    rows, width = kv_own.shape[2], kv_own.shape[3]
    half = width // 2
    piece = min(rows, device_rows)
    pieces = rows // piece
    subs = device_rows // piece
    chunk_shares = CHUNK // rows
    seg_chunks = share_count * rows // CHUNK
    my_head = me // share_count
    my_share = lax.rem(me, share_count)
    core = lax.rem(col, 2)
    place = col // 2
    places = n_tp // 2
    sibling = place * 2 + 1 - core

    loads = [
        pltpu.make_async_copy(src, dst, load_sem.at[index])
        for index, (src, dst) in enumerate(
            [
                (tokens_ref, tok.at[col]),
                (wq_ref, wqkv.at[0]),
                (wk_ref, wqkv.at[1]),
                (wv_ref, wqkv.at[2]),
                (wo_ref, wfull.at[col]),
            ]
        )
    ]
    for copy in loads:
        copy.start()

    barrier = pltpu.get_barrier_semaphore()
    total = n_sp * n_tp
    flat = me * n_tp + col

    def greet(step, carry):
        other = lax.rem(flat + step, total)
        pl.semaphore_signal(
            barrier, inc=1, device_id=(other // n_tp, lax.rem(other, n_tp)), device_id_type=MESH
        )
        return carry

    lax.fori_loop(1, total, greet, 0)
    key_id = lax.broadcasted_iota(jnp.int32, (CHUNK, CHUNK), 0)
    out_id = lax.broadcasted_iota(jnp.int32, (CHUNK, CHUNK), 1)
    tri[...] = jnp.where(key_id > out_id, 1.0, 0.0).astype(jnp.bfloat16)
    pl.semaphore_wait(barrier, total - 1)

    def same_core(k):
        return lax.rem(place + k, places) * 2 + core

    def arrived(ref, sem):
        pltpu.make_async_copy(ref, ref, sem).wait()

    def token_copy(kind, part):
        if kind < places:
            src, block = tokens_ref.at[part], col
            target = sibling if kind == 0 else same_core(kind)
        else:
            block = same_core(kind - places + 1)
            src, target = tok.at[block, part], sibling
        return pltpu.make_async_remote_copy(
            src_ref=src, dst_ref=tok.at[block, part],
            send_sem=tok_send.at[kind, part], recv_sem=tok_recv.at[block, part],
            device_id=(me, target), device_id_type=MESH,
        )

    def wo_copy(kind):
        if kind < places:
            src, block = wo_ref, col
            target = sibling if kind == 0 else same_core(kind)
        else:
            block = same_core(kind - places + 1)
            src, target = wfull.at[block], sibling
        return pltpu.make_async_remote_copy(
            src_ref=src, dst_ref=wfull.at[block],
            send_sem=wo_send.at[kind], recv_sem=wo_recv.at[block],
            device_id=(me, target), device_id_type=MESH,
        )

    for part in range(PARTS):
        for kind in range(places):
            token_copy(kind, part).start()

    lane = lax.broadcasted_iota(jnp.int32, (rows, width), 1)
    lane_half = lax.broadcasted_iota(jnp.int32, (rows // 2, width), 1)

    def turn(value):
        return pltpu.roll(value, half, 1)

    def kv_copy(step, share):
        peer = lax.rem(me + step, n_sp)
        return pltpu.make_async_remote_copy(
            src_ref=kv_own.at[peer // share_count, share], dst_ref=kv_all.at[me, share],
            send_sem=kv_send.at[step, share], recv_sem=kv_recv.at[me, share],
            device_id=(peer, col), device_id_type=MESH,
        )

    def share_of(peer):
        return lax.rem(lax.rem(peer, share_count) + me, share_count)

    def q_copy(step):
        peer = lax.rem(me + step, n_sp)
        return pltpu.make_async_remote_copy(
            src_ref=q_own.at[peer // share_count, share_of(peer)], dst_ref=q_all.at[me],
            send_sem=q_send.at[step], recv_sem=q_recv.at[me],
            device_id=(peer, col), device_id_type=MESH,
        )

    def project(group):
        x = tok[pl.ds(group * pieces, pieces)].reshape(subs * rows, tok.shape[3])
        qf = jnp.dot(x, wqkv[0], preferred_element_type=jnp.float32) * half ** (-0.5)
        kf = jnp.dot(x, wqkv[1], preferred_element_type=jnp.float32)
        vf = jnp.dot(x, wqkv[2], preferred_element_type=jnp.float32)
        for sub in range(subs):
            own = slice(sub * rows, (sub + 1) * rows)
            publish(group * subs + sub, qf[own], kf[own], vf[own])

    def publish(share, qf, kf, vf):
        for pair in range(heads // 2):
            cols = slice(pair * width, (pair + 1) * width)
            kk, vv = kf[:, cols], vf[:, cols]
            top, low = qf[: rows // 2, cols], qf[rows // 2 :, cols]
            kv_own[2 * pair, share] = jnp.where(lane < half, kk, turn(vv)).astype(jnp.bfloat16)
            kv_own[2 * pair + 1, share] = jnp.where(lane < half, turn(kk), vv).astype(jnp.bfloat16)
            q_own[2 * pair, share] = jnp.where(lane_half < half, top, turn(low)).astype(
                jnp.bfloat16
            )
            q_own[2 * pair + 1, share] = jnp.where(lane_half < half, turn(top), low).astype(
                jnp.bfloat16
            )
        for step in range(1, n_sp):
            kv_copy(step, share).start()

            @pl.when(share_of(lax.rem(me + step, n_sp)) == share)
            def _():
                q_copy(step).start()

        kv_all[me, share] = kv_own[my_head, share]

        @pl.when(share_of(me) == share)
        def _():
            q_all[me] = q_own[my_head, share]

    for copy in loads:
        copy.wait()
    own_group = col // pieces
    groups = n_tp // pieces
    if pieces > 1:
        for part in range(PARTS):
            arrived(tok.at[sibling, part], tok_recv.at[sibling, part])
        project(own_group)
    for part in range(PARTS):
        for k in range(1, places):
            block = same_core(k)
            arrived(tok.at[block, part], tok_recv.at[block, part])
            token_copy(places + k - 1, part).start()
    for kind in range(places):
        wo_copy(kind).start()
    for part in range(PARTS):
        if pieces == 1:
            arrived(tok.at[sibling, part], tok_recv.at[sibling, part])
        for k in range(1, places):
            block = lax.rem(place + k, places) * 2 + 1 - core
            arrived(tok.at[block, part], tok_recv.at[block, part])

    def project_next(step, carry):
        project(lax.rem(own_group + step, groups))
        return carry

    lax.fori_loop(1 if pieces > 1 else 0, groups, project_next, 0)

    bias = bias_ref[my_head] * LOG2E

    def logs(q, keys):
        scores = lax.dot_general(
            q, keys, (((1,), (1,)), ((), ())), preferred_element_type=jnp.float32
        )
        z = scores * LOG2E + bias
        log_take = jnp.minimum(z, 0.0) - jnp.log2(1.0 + jnp.exp2(-jnp.abs(z)))
        return log_take, log_take - z

    def tails(keep):
        keep = keep.astype(jnp.bfloat16)
        tail = jnp.dot(keep, tri[...], preferred_element_type=jnp.float32)
        return tail, tail[:, 0:1] + keep[:, 0:1].astype(jnp.float32)

    def chunk_keys(index):
        block, inner = index // seg_chunks, lax.rem(index, seg_chunks)
        return kv_all[block, pl.ds(inner * chunk_shares, chunk_shares)].reshape(CHUNK, width)

    def weigh(log_take, tail, later, keys):
        weight = jnp.exp2(log_take + (tail + later)).astype(jnp.bfloat16)
        return jnp.dot(weight, keys, preferred_element_type=jnp.float32)

    def landing(first_row):
        return (col * heads + my_head) * subs + lax.rem(first_row // piece, subs)

    def is_here(block, index, first_row):
        return jnp.logical_and(block == me, (first_row + index * piece) // device_rows == col)

    def back(block, index, first_row):
        owner = (first_row + index * piece) // device_rows
        slot = landing(first_row)
        return pltpu.make_async_remote_copy(
            src_ref=packed.at[block, index], dst_ref=att.at[slot],
            send_sem=back_send.at[block, index], recv_sem=back_recv.at[slot],
            device_id=(block, owner), device_id_type=MESH,
        )

    def visit(block, carry):
        @pl.when(block != me)
        def _():
            for share in range(share_count):
                arrived(kv_all.at[block, share], kv_recv.at[block, share])
            arrived(q_all.at[block], q_recv.at[block])

        @pl.when(block == n_sp - 2)
        def _():
            for k in range(1, places):
                arrived(wfull.at[same_core(k)], wo_recv.at[same_core(k)])
                wo_copy(places + k - 1).start()

        pair = q_all[block].astype(jnp.float32)
        low = jnp.where(lane_half < half, pair, 0.0)
        high = jnp.where(lane_half < half, turn(pair), 0.0)
        q = jnp.concatenate([low, high], axis=0).astype(jnp.bfloat16)
        first_row = lax.rem(my_share + block, share_count) * rows
        diagonal = first_row // CHUNK
        q_pos = first_row + lax.broadcasted_iota(jnp.int32, (rows, CHUNK), 0)
        k_pos = diagonal * CHUNK + lax.broadcasted_iota(jnp.int32, (rows, CHUNK), 1)
        live = k_pos < q_pos

        keys = chunk_keys(block * seg_chunks + diagonal)
        log_take, keep = logs(q, keys)
        tail, later = tails(jnp.where(live, keep, 0.0))
        weight = jnp.where(live, jnp.exp2(log_take + tail), 0.0).astype(jnp.bfloat16)
        acc = jnp.dot(weight, keys, preferred_element_type=jnp.float32)

        def single(step, state):
            acc, later = state
            keys = chunk_keys(block * seg_chunks + diagonal - 1 - step)
            log_take, keep = logs(q, keys)
            tail, whole = tails(keep)
            return acc + weigh(log_take, tail, later, keys), later + whole

        def segment(step, state):
            acc, later = state
            first = (block - 1 - step) * seg_chunks
            keys = [chunk_keys(first + index) for index in reversed(range(seg_chunks))]
            terms = [logs(q, part) for part in keys]
            ends = [tails(keep) for _, keep in terms]
            for part, (log_take, _), (tail, whole) in zip(keys, terms, ends):
                acc = acc + weigh(log_take, tail, later, part)
                later = later + whole
            return acc, later

        state = lax.fori_loop(0, diagonal, single, (acc, later))
        acc, _ = lax.fori_loop(0, block, segment, state)
        for index in range(pieces):
            top = acc[index * piece : index * piece + piece // 2]
            low = acc[index * piece + piece // 2 : (index + 1) * piece]
            lanes = lax.broadcasted_iota(jnp.int32, top.shape, 1)
            folded = jnp.where(lanes < half, turn(top), low).astype(jnp.bfloat16)
            packed[block, index] = folded
            here = is_here(block, index, first_row)

            @pl.when(here)
            def _():
                att[landing(first_row)] = folded

            @pl.when(jnp.logical_not(here))
            def _():
                back(block, index, first_row).start()

        return carry

    lax.fori_loop(0, n_sp, visit, 0)

    for sub in range(subs):
        share = (col * device_rows + sub * piece) // rows
        source_share = lax.rem(share + n_sp * share_count - me, share_count)
        for source_col in range(n_tp):
            for pair in range(heads // 2):
                values = []
                for head in (2 * pair, 2 * pair + 1):
                    slot = (source_col * heads + head) * subs + sub
                    source = head * share_count + source_share

                    @pl.when(jnp.logical_not(jnp.logical_and(source == me, source_col == col)))
                    def _():
                        arrived(att.at[slot], back_recv.at[slot])

                    values.append(att[slot].astype(jnp.float32))
                lanes = lax.broadcasted_iota(jnp.int32, values[0].shape, 1)
                top = jnp.where(lanes < half, values[0], turn(values[1]))
                low = jnp.where(lanes < half, turn(values[0]), values[1])
                start = (source_col * heads + 2 * pair) * half
                cols = slice(start, start + width)
                middle = sub * piece + piece // 2
                att_rows[sub * piece : middle, cols] = top.astype(jnp.bfloat16)
                att_rows[middle : (sub + 1) * piece, cols] = low.astype(jnp.bfloat16)

    arrived(wfull.at[sibling], wo_recv.at[sibling])
    for k in range(1, places):
        block = lax.rem(place + k, places) * 2 + 1 - core
        arrived(wfull.at[block], wo_recv.at[block])
    for first in range(0, out_ref.shape[1], COLS):
        w = wfull[:, :, first : first + COLS].reshape(att_rows.shape[1], COLS)
        out_ref[:, first : first + COLS] = jnp.dot(
            att_rows[...], w, preferred_element_type=jnp.float32
        ).astype(jnp.bfloat16)

    for kind in range(2 * places - 1):
        wo_copy(kind).wait_send()
        for part in range(PARTS):
            token_copy(kind, part).wait_send()
    for step in range(1, n_sp):
        q_copy(step).wait_send()
        for share in range(share_count):
            kv_copy(step, share).wait_send()

    def drain(block, carry):
        first_row = lax.rem(my_share + block, share_count) * rows
        for index in range(pieces):
            here = is_here(block, index, first_row)

            @pl.when(jnp.logical_not(here))
            def _():
                back(block, index, first_row).wait_send()

        return carry

    lax.fori_loop(0, n_sp, drain, 0)


def shards(tokens, w_query, w_key, w_value, head_bias, w_out):
    model, local_width = w_query.shape
    heads = head_bias.shape[0]
    width = 2 * (local_width // heads)
    n_sp = lax.axis_size("sp")
    n_tp = lax.axis_size("tp")
    device_rows = tokens.shape[0]
    share_count = n_sp // heads
    rows = device_rows * n_tp // share_count
    piece = min(rows, device_rows)
    pieces = rows // piece
    slots = n_tp * heads * device_rows // piece
    out_width = w_out.shape[1]
    places = n_tp // 2
    kinds = 2 * places - 1

    smem = pl.BlockSpec(memory_space=pltpu.SMEM)
    anywhere = pl.BlockSpec(memory_space=pl.ANY)
    dma = pltpu.SemaphoreType.DMA

    def vmem(*shape):
        return pltpu.VMEM(shape, jnp.bfloat16)

    return pl.pallas_call(
        functools.partial(layer_kernel, n_sp, n_tp, heads),
        out_shape=jax.ShapeDtypeStruct((device_rows, out_width), jnp.bfloat16),
        in_specs=[smem] + [anywhere] * 5,
        out_specs=pl.BlockSpec(memory_space=pltpu.VMEM),
        scratch_shapes=[
            vmem(n_tp, PARTS, device_rows // PARTS, model),
            vmem(3, model, local_width),
            vmem(n_tp, local_width, out_width),
            vmem(heads, share_count, rows, width),
            vmem(heads, share_count, rows // 2, width),
            vmem(n_sp, rows // 2, width),
            vmem(n_sp, share_count, rows, width),
            vmem(n_sp, pieces, piece // 2, width),
            vmem(slots, piece // 2, width),
            vmem(device_rows, n_tp * local_width),
            vmem(CHUNK, CHUNK),
            dma((5,)),
            dma((kinds, PARTS)),
            dma((n_tp, PARTS)),
            dma((kinds,)),
            dma((n_tp,)),
            dma((n_sp, share_count)),
            dma((n_sp, share_count)),
            dma((n_sp,)),
            dma((n_sp,)),
            dma((n_sp, pieces)),
            dma((slots,)),
        ],
        compiler_params=pltpu.CompilerParams(
            collective_id=0, has_side_effects=True, vmem_limit_bytes=60 * 2**20
        ),
        name="layer",
    )(
        head_bias,
        tokens.reshape(PARTS, device_rows // PARTS, model),
        w_query, w_key, w_value, w_out,
    )


def solution(mesh):
    placed = (
        P(("sp", "tp"), None),
        P(None, "tp"),
        P(None, "tp"),
        P(None, "tp"),
        P("tp"),
        P("tp", None),
    )
    return jax.shard_map(
        shards, mesh=mesh, in_specs=placed, out_specs=P(("sp", "tp"), None), check_vma=False
    )
```

time: 117 us -> 70.8 us (0.61)
  waiting for transfers between devices: 24.9 us -> 0 us
  between operations: 13.5 us -> 0.01 us
  matrix products: 8.08 us -> 0 us
  Pallas kernels: 64.6 us -> 68.8 us
  local copies, waits for them, and re-layouts: 5.25 us -> 1.88 us
    all_gather x2 -> x0, waiting for transfers between devices: 23.5 us -> none  [the longest x1 23.5 us: shards(): gathered = lax.all_gather(tokens, 'tp', axis=0, tiled=True)]
    dot_general x2 -> x0, matrix products: 8.08 us -> none  [the longest x1 4.38 us: shards(): projected = jnp.dot(gathered, joined, preferred_element_type=jnp.float32)]
    pallas_call x1, Pallas kernels: 64.6 us -> 68.8 us  [shards(): pl.pallas_call(functools.partial(layer_kernel, n_sp, n_tp, heads), out_sh...]
    reshape x8 -> x0, local copies, waits for them, and re-layouts: 3.88 us -> none  [the longest x2 1.53 us: shards(): attended = attended.reshape(n_tp * heads, device_rows // 2, 2, head_size)]
    unnamed x0 -> x1, local copies, waits for them, and re-layouts: none -> 1.88 us
    unnamed x2 -> x0, waiting for transfers between devices: 1.41 us -> none
    dynamic_slice x1 -> x0, local copies, waits for them, and re-layouts: 1.3 us -> none  [shards(): bias = lax.dynamic_slice_in_dim(head_bias, me // share_count, 1, 0)]
  transfers between devices with their start and end apart: 2 -> 0, of which waited for: 1 -> 0; matrix products, arithmetic and copies ran while one was open for 8% -> 0% of each run, Pallas kernels for 55% -> 0%
where the time goes in v2:
time: 70.8 us; the launch traced here: 70.7 us
  Pallas kernels  68.8 us (97%)
  local copies, waits for them, and re-layouts  1.88 us (3%)
    pallas_call x1, Pallas kernels, shards(): pl.pallas_call(functools.partial(layer_kernel, n_sp, n_tp, heads), out_sh...  68.8 us
    unnamed x1, local copies, waits for them, and re-layouts  1.88 us

profile of v2, /device:TPU:29, one launch (start us, length us, event | category | flops | bytes accessed | tf_op | source)
XLA Modules:
  0.0 70.7 jit_solution(11082632408403417643)
XLA Ops:
  0.0 68.8 %layer.1 = bf16[128,2048]{1,0:T(8,128)(2,1)} custom-call(f32[4]{0:T(128)} %bias_ref.1, bf16[4,32,2048]{2,1,0:T(8,128)(2,1)} %bitcast.1, bf16[2048,256]{1,0:T(8,128)(2,1)} %wq_ref.1, bf16[2048,256]{1,0:T(8,128)(2,1)} %wk_ref.1, bf16[2048,256]{1,0:T(8,128)(2,1)} %wv_ref.1, bf16[256,2048]{1,0:T(8,128)(2,1)} %wo_ref.1), custom_call_target="tpu_custom_call" | custom-call | tf_op jit(solution)/shard_map/layer/pallas_call | solution.py:385
  68.8 1.9 %copy.8 = bf16[128,2048]{1,0:T(8,128)(2,1)} copy(bf16[128,2048]{1,0:T(8,128)(2,1)} %layer.1) | data formatting | bytes 1048576

commit v3 on v2

--- a/solution.py
+++ b/solution.py
@@ -13,12 +13,14 @@
 CHUNK = 256
 PARTS = 4
 COLS = 512
+LOOK = 4
+LOG_MAX = 126.0
 
 
 def layer_kernel(
     n_sp, n_tp, heads, bias_ref, tokens_ref, wq_ref, wk_ref, wv_ref, wo_ref, out_ref,
     tok, wqkv, wfull, kv_own, q_own, q_all, kv_all, packed, att, att_rows, tri,
-    load_sem, tok_send, tok_recv, wo_send, wo_recv, kv_send, kv_recv, q_send, q_recv,
+    load_sem, tok_send, tok_recv, wo_send, wo_recv, kv_send, pass_send, kv_recv, q_send, q_recv,
     back_send, back_recv,
 ):
     me = lax.axis_index("sp")
@@ -114,12 +116,27 @@
         return pltpu.roll(value, half, 1)
 
     def kv_copy(step, share):
-        peer = lax.rem(me + step, n_sp)
-        return pltpu.make_async_remote_copy(
-            src_ref=kv_own.at[peer // share_count, share], dst_ref=kv_all.at[me, share],
+        head = lax.rem(my_head + step, heads)
+        return pltpu.make_async_remote_copy(
+            src_ref=kv_own.at[head, share], dst_ref=kv_all.at[me, share],
             send_sem=kv_send.at[step, share], recv_sem=kv_recv.at[me, share],
+            device_id=(head * share_count + my_share, col), device_id_type=MESH,
+        )
+
+    def forward(turn_of, step, share):
+        block = turn_of * share_count + my_share
+        peer = my_head * share_count + lax.rem(my_share + step, share_count)
+        return pltpu.make_async_remote_copy(
+            src_ref=kv_all.at[block, share], dst_ref=kv_all.at[block, share],
+            send_sem=pass_send.at[turn_of, step, share], recv_sem=kv_recv.at[block, share],
             device_id=(peer, col), device_id_type=MESH,
         )
+
+    def relay(block):
+        for share in range(share_count):
+            arrived(kv_all.at[block, share], kv_recv.at[block, share])
+            for step in range(1, share_count):
+                forward(block // share_count, step, share).start()
 
     def share_of(peer):
         return lax.rem(lax.rem(peer, share_count) + me, share_count)
@@ -134,7 +151,7 @@
 
     def project(group):
         x = tok[pl.ds(group * pieces, pieces)].reshape(subs * rows, tok.shape[3])
-        qf = jnp.dot(x, wqkv[0], preferred_element_type=jnp.float32) * half ** (-0.5)
+        qf = jnp.dot(x, wqkv[0], preferred_element_type=jnp.float32) * (LOG2E * half ** (-0.5))
         kf = jnp.dot(x, wqkv[1], preferred_element_type=jnp.float32)
         vf = jnp.dot(x, wqkv[2], preferred_element_type=jnp.float32)
         for sub in range(subs):
@@ -154,14 +171,16 @@
             q_own[2 * pair + 1, share] = jnp.where(lane_half < half, turn(top), low).astype(
                 jnp.bfloat16
             )
+        for step in range(1, heads):
+            kv_copy(step, share).start()
+        kv_all[me, share] = kv_own[my_head, share]
+        for step in range(1, share_count):
+            forward(my_head, step, share).start()
         for step in range(1, n_sp):
-            kv_copy(step, share).start()
 
             @pl.when(share_of(lax.rem(me + step, n_sp)) == share)
             def _():
                 q_copy(step).start()
-
-        kv_all[me, share] = kv_own[my_head, share]
 
         @pl.when(share_of(me) == share)
         def _():
@@ -201,22 +220,24 @@
         scores = lax.dot_general(
             q, keys, (((1,), (1,)), ((), ())), preferred_element_type=jnp.float32
         )
-        z = scores * LOG2E + bias
-        log_take = jnp.minimum(z, 0.0) - jnp.log2(1.0 + jnp.exp2(-jnp.abs(z)))
-        return log_take, log_take - z
-
-    def tails(keep):
-        keep = keep.astype(jnp.bfloat16)
-        tail = jnp.dot(keep, tri[...], preferred_element_type=jnp.float32)
-        return tail, tail[:, 0:1] + keep[:, 0:1].astype(jnp.float32)
+        z = scores + bias
+        lose = jnp.maximum(
+            jnp.log(1.0 + jnp.exp2(jnp.minimum(z, LOG_MAX))) * LOG2E, z
+        )
+        return z - lose, lose
+
+    def tails(lose):
+        lose = lose.astype(jnp.bfloat16)
+        tail = jnp.dot(lose, tri[...], preferred_element_type=jnp.float32)
+        return tail, tail[:, 0:1] + lose[:, 0:1].astype(jnp.float32)
 
     def chunk_keys(index):
         block, inner = index // seg_chunks, lax.rem(index, seg_chunks)
         return kv_all[block, pl.ds(inner * chunk_shares, chunk_shares)].reshape(CHUNK, width)
 
     def weigh(log_take, tail, later, keys):
-        weight = jnp.exp2(log_take + (tail + later)).astype(jnp.bfloat16)
-        return jnp.dot(weight, keys, preferred_element_type=jnp.float32)
+        weight = jnp.exp2(log_take - tail).astype(jnp.bfloat16)
+        return jnp.exp2(-later) * jnp.dot(weight, keys, preferred_element_type=jnp.float32)
 
     def landing(first_row):
         return (col * heads + my_head) * subs + lax.rem(first_row // piece, subs)
@@ -233,11 +254,29 @@
             device_id=(block, owner), device_id_type=MESH,
         )
 
+    def relayed(block):
+        return jnp.logical_and(lax.rem(block, share_count) == my_share, block != me)
+
+    for block in range(LOOK):
+
+        @pl.when(relayed(block))
+        def _():
+            relay(block)
+
     def visit(block, carry):
-        @pl.when(block != me)
+        ahead = block + LOOK
+
+        @pl.when(jnp.logical_and(ahead < n_sp, relayed(ahead)))
+        def _():
+            relay(ahead)
+
+        @pl.when(lax.rem(block, share_count) != my_share)
         def _():
             for share in range(share_count):
                 arrived(kv_all.at[block, share], kv_recv.at[block, share])
+
+        @pl.when(block != me)
+        def _():
             arrived(q_all.at[block], q_recv.at[block])
 
         @pl.when(block == n_sp - 2)
@@ -259,7 +298,7 @@
         keys = chunk_keys(block * seg_chunks + diagonal)
         log_take, keep = logs(q, keys)
         tail, later = tails(jnp.where(live, keep, 0.0))
-        weight = jnp.where(live, jnp.exp2(log_take + tail), 0.0).astype(jnp.bfloat16)
+        weight = jnp.where(live, jnp.exp2(log_take - tail), 0.0).astype(jnp.bfloat16)
         acc = jnp.dot(weight, keys, preferred_element_type=jnp.float32)
 
         def single(step, state):
@@ -342,8 +381,12 @@
             token_copy(kind, part).wait_send()
     for step in range(1, n_sp):
         q_copy(step).wait_send()
-        for share in range(share_count):
+    for share in range(share_count):
+        for step in range(1, heads):
             kv_copy(step, share).wait_send()
+        for turn_of in range(heads):
+            for step in range(1, share_count):
+                forward(turn_of, step, share).wait_send()
 
     def drain(block, carry):
         first_row = lax.rem(my_share + block, share_count) * rows
@@ -404,7 +447,8 @@
             dma((n_tp, PARTS)),
             dma((kinds,)),
             dma((n_tp,)),
-            dma((n_sp, share_count)),
+            dma((heads, share_count)),
+            dma((heads, share_count, share_count)),
             dma((n_sp, share_count)),
             dma((n_sp,)),
             dma((n_sp,)),

time: 70.8 us -> 65.8 us (0.929)
  Pallas kernels: 68.8 us -> 63.3 us
    pallas_call x1, Pallas kernels: 68.8 us -> 63.3 us  [shards(): pl.pallas_call(functools.partial(layer_kernel, n_sp, n_tp, heads), out_sh...]
where the time goes in v3:
time: 65.8 us; the launch traced here: 65.2 us
  Pallas kernels  63.3 us (96%)
  local copies, waits for them, and re-layouts  1.88 us (3%)
    pallas_call x1, Pallas kernels, shards(): pl.pallas_call(functools.partial(layer_kernel, n_sp, n_tp, heads), out_sh...  63.3 us
    unnamed x1, local copies, waits for them, and re-layouts  1.88 us

profile of v3, /device:TPU:29, one launch (start us, length us, event | category | flops | bytes accessed | tf_op | source)
XLA Modules:
  0.0 65.2 jit_solution(1550106142867013567)
XLA Ops:
  0.0 63.3 %layer.1 = bf16[128,2048]{1,0:T(8,128)(2,1)} custom-call(f32[4]{0:T(128)} %bias_ref.1, bf16[4,32,2048]{2,1,0:T(8,128)(2,1)} %bitcast.1, bf16[2048,256]{1,0:T(8,128)(2,1)} %wq_ref.1, bf16[2048,256]{1,0:T(8,128)(2,1)} %wk_ref.1, bf16[2048,256]{1,0:T(8,128)(2,1)} %wv_ref.1, bf16[256,2048]{1,0:T(8,128)(2,1)} %wo_ref.1), custom_call_target="tpu_custom_call" | custom-call | tf_op jit(solution)/shard_map/layer/pallas_call | solution.py:428
  63.3 1.9 %copy.8 = bf16[128,2048]{1,0:T(8,128)(2,1)} copy(bf16[128,2048]{1,0:T(8,128)(2,1)} %layer.1) | data formatting | bytes 1048576
